TPU v7x, 32 devices: a whole 2x2x4 slice. The times are simulated.
32 devices in a mesh: sp: 8 (over z, x), tp: 4 (over y, core).
Axes of the slice: x: 2, y: 2, z: 4, core: 2. Of those that a mesh axis runs over, the one named last changes fastest.
Arguments:
- skip_stream_entering: bfloat16 [1024, 2048], P('sp', 'tp'), may hold values from -24 to 24
- unfiltered_channel_feed: bfloat16 [1024, 2048], P('sp', 'tp'), may hold values from -6 to 6
- unfiltered_state_entry: bfloat16 [1024, 2048], P('sp', 'tp'), may hold values from -6 to 6
- unfiltered_state_exit: bfloat16 [1024, 2048], P('sp', 'tp'), may hold values from -6 to 6
- final_valve_preactivation: bfloat16 [1024, 2048], P('sp', 'tp'), may hold values from -6 to 6
- increment_preactivation: float32 [2, 32, 1024], P(None, 'tp', 'sp'), may hold values from -8 to 8
- summed_attenuation_both_ways: float32 [2, 32, 1024], P(None, 'tp', 'sp'), may hold values from -0.7 to 0, as said below
- channel_fading_speed: float32 [2, 32], P(None, 'tp'), may hold values from 0.0001953125 to 0.03, as said below
- channel_feed_filter: float32 [5, 2048], P(None, 'tp'), may hold values from -2.5 to 2.5
- state_entry_filter: float32 [5, 2048], P(None, 'tp'), may hold values from -2.5 to 2.5
- state_exit_filter: float32 [5, 2048], P(None, 'tp'), may hold values from -2.5 to 2.5
- clustered_rescale_factor: float32 [2048], P('tp'), may hold values from 0.1 to 1.9
- final_projection_weights: bfloat16 [2048, 2048], P(None, 'tp'), may hold values from -0.125 to 0.125
- specialist_rescale_factor: float32 [2048], replicated, may hold values from 0.1 to 1.9
- item_specialist_couple: int32 [1024, 2], P('sp'), may hold values from 0 to 7, all different within a row; in each aligned block of 128 rows (0 to 127, 128 to 255, ...) at most 64 rows name the same one
- selected_cluster_likelihood: float32 [1024], P('sp'), may hold values from 0.3 to 1
- selected_twin_scores_raw: float32 [1024, 2], P('sp'), may hold values from -6 to 6
- specialist_gating_weights: bfloat16 [8, 2048, 4096], P('sp', None, 'tp'), may hold values from -0.125 to 0.125
- specialist_raising_weights: bfloat16 [8, 2048, 4096], P('sp', None, 'tp'), may hold values from -0.125 to 0.125
- specialist_lowering_weights: bfloat16 [8, 4096, 2048], P('sp', 'tp'), may hold values from -0.09375 to 0.09375
Outputs:
- layer_out: bfloat16 [1024, 2048], P('sp', 'tp')
Inputs may be any that keep to these rules, and one draw needn't show every extreme that they name: For every head, dt times channel_fading_speed at the rate of the draw sets how far a state is carried; summed_attenuation_both_ways holds a few sharp losses of state. `summed_attenuation_both_ways`: mostly zero. `item_specialist_couple`: the two experts of a row differ. Among the rows of one index of sp (aligned blocks of 128 rows) no expert is named by more than 64 rows, a bound that some expert reaches in some blocks.
All inputs are finite; a program needn't handle non-finite values.
Results may differ from a plain program's by a relative error of at most 0.0095.
Values may be sent and summed in bfloat16 or wider, within the bound.
A program may use at most 64 MiB of HBM per device.

v0:
```python
import jax
import jax.numpy as jnp
from jax import lax
from jax.sharding import PartitionSpec as P

D = 2048
HD = 64
NS = 128
CONV = 5


HIGHEST = lax.Precision.HIGHEST
group_eps = 1e-05
stream_eps = 1e-06


def extended(cells, sides, width):
    for axis, dim in sides:
        count = lax.axis_size(axis)
        ends = count - 1
        head = lax.slice_in_dim(cells, 0, width, axis=dim)
        tail = lax.slice_in_dim(cells, cells.shape[dim] - width, cells.shape[dim], axis=dim)
        cells = jnp.concatenate(
            [
                lax.ppermute(tail, axis, [(i, (i + 1) % count) for i in range(ends)]),
                cells,
                lax.ppermute(head, axis, [((i + 1) % count, i) for i in range(ends)]),
            ],
            axis=dim,
        )
    return cells


def entering(shard, axis, join, neutral, backward):
    count = lax.axis_size(axis)
    place = lax.axis_index(axis)
    ahead = count - 1 - place if backward else place
    gathered = jax.tree.map(
        lambda a, kind: lax.all_gather(a.astype(kind), axis), shard, (jnp.bfloat16, jnp.bfloat16)
    )
    state = jax.tree.map(lambda a, e: jnp.zeros_like(a) + jnp.asarray(e, a.dtype), shard, neutral)

    def one(turn, state):
        source = count - 1 - turn if backward else turn
        return join(
            state,
            jax.tree.map(
                lambda a, own: lax.dynamic_index_in_dim(a, source, 0, False).astype(own.dtype),
                gathered,
                shard,
            ),
        )

    return lax.fori_loop(0, ahead, one, state)


def block_parts(x_short, b_short, c_short, step_f, step_b, log_f, log_b):
    head_count = x_short.shape[1]
    group_count = b_short.shape[1]
    per_group = head_count // group_count
    length = x_short.shape[0]
    group_scores = jnp.einsum("tgn,sgn->gts", c_short, b_short, preferred_element_type=jnp.float32)
    x_block = x_short.astype(jnp.float32)
    b_block = b_short.astype(jnp.float32)
    c_block = c_short.astype(jnp.float32)
    scores = jnp.repeat(group_scores, per_group, axis=0)
    b_head = jnp.repeat(b_block, per_group, axis=1)
    c_head = jnp.repeat(c_block, per_group, axis=1)
    forward = jnp.cumsum(log_f, axis=1)
    backward = jnp.flip(jnp.cumsum(jnp.flip(log_b, 1), axis=1), 1)
    row_index = lax.broadcasted_iota(jnp.int32, (length, length), 0)
    col_index = lax.broadcasted_iota(jnp.int32, (length, length), 1)
    lower_mask = (col_index <= row_index)[None]
    upper_mask = (col_index >= row_index)[None]
    decay_fwd = jnp.where(
        lower_mask, jnp.exp(jnp.minimum(forward[:, :, None] - forward[:, None, :], 0.0)), 0.0
    )
    decay_bwd = jnp.where(
        upper_mask, jnp.exp(jnp.minimum(backward[:, :, None] - backward[:, None, :], 0.0)), 0.0
    )
    mixing = scores * (decay_fwd * step_f[:, None, :] + decay_bwd * step_b[:, None, :])
    within = jnp.einsum("hts,shp->thp", mixing, x_block, precision=HIGHEST)
    weight_fwd = jnp.exp(forward[:, -1:] - forward) * step_f
    weight_bwd = jnp.exp(backward[:, :1] - backward) * step_b
    state_fwd = jnp.einsum("hs,shp,shn->hpn", weight_fwd, x_block, b_head, precision=HIGHEST)
    state_bwd = jnp.einsum("hs,shp,shn->hpn", weight_bwd, x_block, b_head, precision=HIGHEST)
    return (
        within,
        state_fwd,
        state_bwd,
        forward[:, -1],
        backward[:, 0],
        jnp.exp(forward),
        jnp.exp(backward),
        c_head,
    )


def read_state(c_head, factor, state):
    return (
        jnp.einsum("thn,hpn->thp", c_head, state, precision=HIGHEST)
        * jnp.transpose(factor)[:, :, None]
    )


def compose(earlier, later):
    return (earlier[0] + later[0], earlier[1] * jnp.exp(later[0])[:, None, None] + later[1])


def body(
    skip_stream_entering,
    unfiltered_channel_feed,
    unfiltered_state_entry,
    unfiltered_state_exit,
    final_valve_preactivation,
    increment_preactivation,
    summed_attenuation_both_ways,
    channel_fading_speed,
    channel_feed_filter,
    state_entry_filter,
    state_exit_filter,
    clustered_rescale_factor,
    final_projection_weights,
    specialist_rescale_factor,
    item_specialist_couple,
    selected_cluster_likelihood,
    selected_twin_scores_raw,
    specialist_gating_weights,
    specialist_raising_weights,
    specialist_lowering_weights,
):
    tokens_here = skip_stream_entering.shape[0]
    heads_here = increment_preactivation.shape[1]
    x_width = unfiltered_channel_feed.shape[1]
    b_width = unfiltered_state_entry.shape[1]
    groups_here = b_width // NS
    joined = jnp.concatenate(
        [unfiltered_channel_feed, unfiltered_state_entry, unfiltered_state_exit], axis=1
    )
    padded = extended(joined, (("sp", 0),), CONV // 2)
    kernel = jnp.concatenate([channel_feed_filter, state_entry_filter, state_exit_filter], axis=1)
    summed = jnp.zeros(joined.shape, jnp.float32)
    for offset in range(CONV):
        summed = summed + kernel[offset] * padded[offset : offset + tokens_here].astype(jnp.float32)
    conv_out = jax.nn.silu(summed).astype(jnp.bfloat16)
    x_conv = conv_out[:, :x_width].reshape(tokens_here, heads_here, HD)
    b_conv = conv_out[:, x_width : x_width + b_width].reshape(tokens_here, groups_here, NS)
    c_conv = conv_out[:, x_width + b_width :].reshape(tokens_here, groups_here, NS)
    whole_increment_list = jax.nn.softplus(increment_preactivation)
    whole_attenuation_list = (
        -whole_increment_list * channel_fading_speed[:, :, None] + summed_attenuation_both_ways
    )
    within, state_fwd, state_bwd, total_fwd, total_bwd, factor_fwd, factor_bwd, c_head = (
        block_parts(
            x_conv,
            b_conv,
            c_conv,
            whole_increment_list[0],
            whole_increment_list[1],
            whole_attenuation_list[0],
            whole_attenuation_list[1],
        )
    )
    empty = (jnp.zeros_like(total_fwd), jnp.zeros_like(state_fwd))
    incoming_fwd = entering((total_fwd, state_fwd), "sp", compose, empty, False)[1]
    incoming_bwd = entering((total_bwd, state_bwd), "sp", compose, empty, True)[1]
    mixer_out = (
        within
        + read_state(c_head, factor_fwd, incoming_fwd)
        + read_state(c_head, factor_bwd, incoming_bwd)
    )
    gated = mixer_out.reshape(tokens_here, x_width) * jax.nn.silu(
        final_valve_preactivation.astype(jnp.float32)
    )
    grouped = gated.reshape(tokens_here, groups_here, -1)
    grouped = grouped * lax.rsqrt(jnp.mean(grouped * grouped, axis=-1, keepdims=True) + group_eps)
    mixed = (grouped.reshape(tokens_here, x_width) * clustered_rescale_factor).astype(jnp.bfloat16)
    projected = jnp.dot(
        lax.all_gather(mixed, "tp", axis=1, tiled=True),
        final_projection_weights,
        preferred_element_type=jnp.float32,
    )
    stream = (skip_stream_entering.astype(jnp.float32) + projected).astype(jnp.bfloat16)
    stream_f = stream.astype(jnp.float32)
    col_count = skip_stream_entering.shape[1]
    squares = lax.psum(jnp.sum(stream_f * stream_f, axis=1), "tp")
    row_scale = lax.rsqrt(squares / D + stream_eps)
    gain_cols = lax.dynamic_slice_in_dim(
        specialist_rescale_factor, lax.axis_index("tp") * col_count, col_count, 0
    )
    normal_cols = (stream_f * row_scale[:, None] * gain_cols).astype(jnp.bfloat16)
    expert_total = lax.axis_size("sp")
    capacity = 4 * tokens_here // expert_total
    flat_ids = item_specialist_couple.reshape(-1)
    assignments = flat_ids.shape[0]
    expert_iota = lax.broadcasted_iota(jnp.int32, (assignments, expert_total), 1)
    one_hot = (flat_ids[:, None] == expert_iota).astype(jnp.int32)
    ranking = jnp.sum((jnp.cumsum(one_hot, axis=0) - 1) * one_hot, axis=1)
    slot_index = flat_ids * capacity + ranking
    slot_iota = lax.broadcasted_iota(jnp.int32, (expert_total * capacity, assignments), 0)
    selector = (slot_index[None, :] == slot_iota).astype(jnp.bfloat16)
    selector = jnp.sum(selector.reshape(expert_total * capacity, tokens_here, -1), axis=2)
    weight_gate = specialist_gating_weights[0]
    weight_up = specialist_raising_weights[0]
    weight_down = specialist_lowering_weights[0]
    outgoing = jnp.dot(selector, normal_cols, preferred_element_type=jnp.float32).astype(
        jnp.bfloat16
    )
    outgoing = outgoing.reshape(expert_total, capacity, col_count)
    arrived = lax.all_gather(
        lax.all_to_all(outgoing, "sp", split_axis=0, concat_axis=0, tiled=True),
        "tp",
        axis=2,
        tiled=True,
    )
    sources = arrived.shape[0]
    slot_count = arrived.shape[1]
    rows = arrived.reshape(sources * slot_count, arrived.shape[2])
    gate = jnp.dot(rows, weight_gate, preferred_element_type=jnp.float32)
    upward = jnp.dot(rows, weight_up, preferred_element_type=jnp.float32)
    hidden = (jax.nn.silu(gate) * upward).astype(jnp.bfloat16)
    partial_out = jnp.dot(hidden, weight_down, preferred_element_type=jnp.float32).astype(
        jnp.bfloat16
    )
    partial_out = partial_out.reshape(sources, slot_count, partial_out.shape[1])
    expert_cols = (
        lax.psum_scatter(partial_out, "tp", scatter_dimension=2, tiled=True)
        .astype(jnp.float32)
        .astype(jnp.bfloat16)
    )
    returned = lax.all_to_all(expert_cols, "sp", split_axis=0, concat_axis=0, tiled=True)
    flat_back = returned.reshape(expert_total * capacity, col_count)
    picked = (
        jnp.take(flat_back, slot_index, axis=0)
        .astype(jnp.float32)
        .reshape(tokens_here, -1, col_count)
    )
    first = jax.nn.sigmoid(selected_twin_scores_raw[:, 0] - selected_twin_scores_raw[:, 1])
    route_weight = selected_cluster_likelihood[:, None] * jnp.stack([first, 1.0 - first], axis=1)
    experts_sum = jnp.sum(route_weight[:, :, None] * picked, axis=1)
    return (stream_f + experts_sum).astype(jnp.bfloat16)


def solution(mesh):
    placed = (
        P("sp", "tp"),
        P("sp", "tp"),
        P("sp", "tp"),
        P("sp", "tp"),
        P("sp", "tp"),
        P(None, "tp", "sp"),
        P(None, "tp", "sp"),
        P(None, "tp"),
        P(None, "tp"),
        P(None, "tp"),
        P(None, "tp"),
        P("tp"),
        P(None, "tp"),
        P(),
        P("sp", None),
        P("sp"),
        P("sp", None),
        P("sp", None, "tp"),
        P("sp", None, "tp"),
        P("sp", "tp", None),
    )
    return jax.shard_map(body, mesh=mesh, in_specs=placed, out_specs=P("sp", "tp"), check_vma=False)
```

profile of v0, /device:TPU:0, one launch (start us, length us, event | category | flops | bytes accessed | tf_op | source)
XLA Modules:
  0.0 269.3 jit_solution(7861130468680984033)
XLA Ops:
  6.6 1.2 copy.78
  10.1 5.6 %collective-permute-start = (bf16[2,1536]{0,1:T(8,128)(2,1)S(1)}, bf16[2,1536]{0,1:T(8,128)(2,1)}, u32[]{:S(2)}, u32[]{:S(2)}) collective-permute-start(bf16[2,1536]{0,1:T(8,128)(2,1)S(1)} %get-tuple-element.171), channel_id=1, source_target_pairs={{0,4},{4,8},{8,12},{12,16},{16,20},{20,24},{24,28},{1,5},{5,9},{9,... | collective-permute-start | bytes 18440 | tf_op jit(solution)/shard_map/ppermute | solution.py:25
  15.7 1.3 collective-permute-start.1
  18.4 13.3 %collective-permute-done = bf16[2,1536]{0,1:T(8,128)(2,1)} collective-permute-done((bf16[2,1536]{0,1:T(8,128)(2,1)S(1)}, bf16[2,1536]{0,1:T(8,128)(2,1)}, u32[]{:S(2)}, u32[]{:S(2)}) %collective-permute-start) | collective-permute-done | bytes 6176 | tf_op jit(solution)/shard_map/ppermute | solution.py:25
  31.7 1.6 maximum_maximum_fusion
  33.3 3.4 %multiply_convert_fusion.1 = bf16[128,1536]{0,1:T(8,128)(2,1)S(1)} fusion(bf16[130,1536]{0,1:T(8,128)(2,1)S(1)} %get-tuple-element.170, bf16[130,1536]{0,1:T(8,128)(2,1)S(1)} %get-tuple-element.169, f32[1536]{0:T(1024)S(1)} %get-tuple-element.136, f32[1536]{0:T(1024)S(1)} %get-tuple-element.137, f32[1536]{0:T(1024)S(1)} %get-tuple-element.138, ...), kind=kLoop, calls=%fused_computation.28 | loop fusion | flops 4718592 | bytes 2390016 | tf_op jit(solution)/shard_map/convert_element_type | solution.py:145
  36.9 1.2 convolution_convert_fusion.2
  40.8 21.6 %all-reduce.2 = (bf16[64]{0:T(256)(128)(2,1)S(1)}, bf16[64]{0:T(256)(128)(2,1)S(1)}) all-reduce(bf16[64]{0:T(256)(128)(2,1)S(1)} %dynamic-update-slice.1, bf16[64]{0:T(256)(128)(2,1)S(1)} %dynamic-update-slice), channel_id=4, replica_groups=mesh['sp'=8,'tp'=4] {'sp'}, use_global_device_ids=true, to_apply=%add.1 | all-reduce | flops 128 | bytes 512
  64.3 1.4 dynamic_slice.29
  66.2 1.3 convolution_convert_fusion.1
  69.0 12.0 %all-gather.10.cloned.1.call-done = bf16[64,64,128]{2,1,0:T(8,128)(2,1)} async-done(((bf16[8,64,128]{2,1,0:T(8,128)(2,1)}), bf16[64,64,128]{2,1,0:T(8,128)(2,1)}) %all-gather.10.cloned.1.call-update) | async-done | bytes 1048592 | tf_op jit(solution)/shard_map/all_gather | solution.py:39
  81.0 41.1 %all-gather.12.cloned.1.call-done = bf16[64,64,128]{2,1,0:T(8,128)(2,1)} async-done(((bf16[8,64,128]{2,1,0:T(8,128)(2,1)}), bf16[64,64,128]{2,1,0:T(8,128)(2,1)}) %all-gather.12.cloned.1.call-update) | async-done | bytes 1048592 | tf_op jit(solution)/shard_map/all_gather | solution.py:39
  122.2 12.1 %while.27 = (s32[]{:T(128)}, f32[8,64,128]{2,1,0:T(8,128)S(1)}, s32[]{:T(128)}, bf16[8,8]{1,0:T(8,128)(2,1)}, bf16[8,8,64,128]{3,2,1,0:T(8,128)(2,1)}, /*index=5*/s32[]{:T(128)}, s32[]{:T(128)}, s32[]{:T(128)}, s32[]{:T(128)}) while((s32[]{:T(128)}, f32[8,64,128]{2,1,0:T(8,128)S(1)}, s32[]{:T(128)}, bf16[8,8]{1,0:T(8,128)(2,1)}, ...), condition=%wide.region_5.6_spmd, body=%wide.region_4.5_spmd.sunk | while | flops 196622 | bytes 655587 | solution.py:54
  134.3 1.1 fusion.12
  139.1 7.2 %all_gather.32 = bf16[128,2048]{1,0:T(8,128)(2,1)S(1)} all-gather(bf16[128,512]{1,0:T(8,128)(2,1)S(1)} %fusion.26), channel_id=1, replica_groups=mesh['sp'=8,'tp'=4] {'tp'}, dimensions={1}, use_global_device_ids=true | all-gather | bytes 655360 | tf_op jit(solution)/shard_map/all_gather | solution.py:179
  146.8 6.4 %psum.7 = f32[128]{0:T(128)S(1)} all-reduce(f32[128]{0:T(128)S(1)} %get-tuple-element.183), channel_id=1, replica_groups=mesh['sp'=8,'tp'=4] {'tp'}, use_global_device_ids=true, to_apply=%region_12.13 | all-reduce | flops 128 | bytes 1024 | tf_op jit(solution)/shard_map/psum | solution.py:186
  153.6 17.1 %all_to_all.10 = bf16[8,64,512]{2,1,0:T(8,128)(2,1)} all-to-all(bf16[8,64,512]{2,1,0:T(8,128)(2,1)S(1)} %bitcast.118), channel_id=1, replica_groups=mesh['sp'=8,'tp'=4] {'sp'}, dimensions={0} | all-to-all | bytes 1048576 | tf_op jit(solution)/shard_map/all_to_all | solution.py:211
  170.9 20.9 %all-gather.8.cloned.1.call-done = bf16[8,64,2048]{2,1,0:T(8,128)(2,1)} async-done(((bf16[8,64,512]{2,1,0:T(8,128)(2,1)}), bf16[8,64,2048]{2,1,0:T(8,128)(2,1)}) %all-gather.8.cloned.1.call-update) | async-done | bytes 2097168 | tf_op jit(solution)/shard_map/all_gather | solution.py:210
  191.8 6.5 %fusion.4 = f32[512,1024]{1,0:T(8,128)} fusion(bf16[512,2048]{1,0:T(8,128)(2,1)} %bitcast.132, bf16[1,2048,1024]{2,1,0:T(8,128)(2,1)} %param.41), kind=kOutput, calls=%fused_computation.9 | convolution fusion | flops 2147483648 | bytes 8388608 | tf_op jit(solution)/shard_map/dot_general | solution.py:219
  198.3 10.5 %fusion.6 = bf16[512,2048]{1,0:T(8,128)(2,1)} fusion(bf16[1,1024,2048]{2,1,0:T(8,128)(2,1)} %param.43, f32[512,1024]{1,0:T(8,128)} %fusion.4, bf16[512,2048]{1,0:T(8,128)(2,1)} %bitcast.133, bf16[1,2048,1024]{2,1,0:T(8,128)(2,1)} %param.42), kind=kOutput, calls=%fused_computation.11 | convolution fusion | flops 4299161600 | bytes 14680064 | tf_op jit(solution)/shard_map/dot_general | solution.py:222
  208.8 31.3 %reduce-scatter.2.cloned.1.call-done = bf16[8,64,512]{2,1,0:T(8,128)(2,1)} async-done(((bf16[8,64,2048]{2,1,0:T(8,128)(2,1)}), bf16[8,64,512]{2,1,0:T(8,128)(2,1)}) %reduce-scatter.2.cloned.1.call-update) | async-done | bytes 524304 | tf_op jit(solution)/shard_map/reduce_scatter | solution.py:227
  240.2 5.5 %all-to-all-start.1 = ((bf16[8,64,512]{2,1,0:T(8,128)(2,1)}), bf16[8,64,512]{2,1,0:T(8,128)(2,1)S(1)}, u32[]{:S(2)}, u32[]{:S(2)}) async-start(bf16[8,64,512]{2,1,0:T(8,128)(2,1)} %reduce-scatter.2.cloned.1.call-done), calls=%async_computation.2 | async-start | bytes 1048576 | tf_op jit(solution)/shard_map/all_to_all | solution.py:231
  246.3 13.7 %all-to-all-done.1 = bf16[8,64,512]{2,1,0:T(8,128)(2,1)S(1)} async-done(((bf16[8,64,512]{2,1,0:T(8,128)(2,1)}), bf16[8,64,512]{2,1,0:T(8,128)(2,1)S(1)}, u32[]{:S(2)}, u32[]{:S(2)}) %all-to-all-start.1) | async-done | bytes 524320 | tf_op jit(solution)/shard_map/all_to_all | solution.py:231
  260.0 1.2 gather_fusion
  (131 shorter events, 28.5 us)
Async XLA Ops:
  6.5 139.7 %copy-start = (bf16[2048,512]{1,0:T(8,128)(2,1)S(1)}, bf16[2048,512]{1,0:T(8,128)(2,1)}, u32[]{:S(2)}) copy-start(bf16[2048,512]{1,0:T(8,128)(2,1)} %param.36) | copy-start | bytes 6291460
  6.5 10.4 %copy-start.9 = (f32[2,8,128]{2,1,0:T(8,128)S(1)}, f32[2,8,128]{2,1,0:T(8,128)}, u32[]{:S(2)}) copy-start(f32[2,8,128]{2,1,0:T(8,128)} %param.29) | copy-start | bytes 24580
  6.5 10.4 %copy-start.10 = (f32[2,8,128]{2,1,0:T(8,128)S(1)}, f32[2,8,128]{2,1,0:T(8,128)}, u32[]{:S(2)}) copy-start(f32[2,8,128]{2,1,0:T(8,128)} %param.30) | copy-start | bytes 24580
  6.5 10.4 %copy-start.13 = (f32[2,8]{1,0:T(2,128)S(1)}, f32[2,8]{1,0:T(2,128)}, u32[]{:S(2)}) copy-start(f32[2,8]{1,0:T(2,128)} %param.31) | copy-start | bytes 196
  6.5 11.1 %copy-start.4 = (f32[5,512]{1,0:T(8,128)S(1)}, f32[5,512]{1,0:T(8,128)}, u32[]{:S(2)}) copy-start(f32[5,512]{1,0:T(8,128)} %param.32) | copy-start | bytes 30724
  6.5 11.6 %copy-start.5 = (f32[5,512]{1,0:T(8,128)S(1)}, f32[5,512]{1,0:T(8,128)}, u32[]{:S(2)}) copy-start(f32[5,512]{1,0:T(8,128)} %param.33) | copy-start | bytes 30724
  6.6 11.6 %copy-start.6 = (f32[5,512]{1,0:T(8,128)S(1)}, f32[5,512]{1,0:T(8,128)}, u32[]{:S(2)}) copy-start(f32[5,512]{1,0:T(8,128)} %param.34) | copy-start | bytes 30724
  6.6 74.4 %all-gather.10.cloned.1.call-start = ((), (), s32[]{:S(2)}) async-start(), calls=%async_computation.5 | async-start | bytes 1179648 | tf_op jit(solution)/shard_map/all_gather | solution.py:39
  10.1 21.7 %collective-permute-start = (bf16[2,1536]{0,1:T(8,128)(2,1)S(1)}, bf16[2,1536]{0,1:T(8,128)(2,1)}, u32[]{:S(2)}, u32[]{:S(2)}) collective-permute-start(bf16[2,1536]{0,1:T(8,128)(2,1)S(1)} %get-tuple-element.171), channel_id=1, source_target_pairs={{0,4},{4,8},{8,12},{12,16},{16,20},{20,24},{24,28},{1,5},{5,9},{9,... | collective-permute-start | bytes 18440 | tf_op jit(solution)/shard_map/ppermute | solution.py:25
  15.7 16.0 %collective-permute-start.1 = (bf16[2,1536]{0,1:T(8,128)(2,1)S(1)}, bf16[2,1536]{0,1:T(8,128)(2,1)}, u32[]{:S(2)}, u32[]{:S(2)}) collective-permute-start(bf16[2,1536]{0,1:T(8,128)(2,1)S(1)} %get-tuple-element.172), channel_id=1, source_target_pairs={{4,0},{8,4},{12,8},{16,12},{20,16},{24,20},{28,24},{5,1},{9,5},{13... | collective-permute-start | bytes 18440 | tf_op jit(solution)/shard_map/ppermute | solution.py:27
  33.3 5.0 %copy-start.7 = (s32[128,2]{0,1:T(2,128)S(1)}, s32[128,2]{0,1:T(2,128)}, u32[]{:S(2)}) copy-start(s32[128,2]{0,1:T(2,128)} %param.38) | copy-start | bytes 3076
  36.7 2.0 copy-start.16
  38.2 83.9 %all-gather.12.cloned.1.call-start = ((), (), s32[]{:S(2)}) async-start(), calls=%async_computation.6 | async-start | bytes 1179648 | tf_op jit(solution)/shard_map/all_gather | solution.py:39
  67.5 124.3 %all-gather.8.cloned.1.call-start = ((), (), s32[]{:S(2)}) async-start(), calls=%async_computation.3 | async-start | bytes 2621440 | tf_op jit(solution)/shard_map/all_gather | solution.py:210
  136.6 2.3 copy-start.2
  136.6 2.3 copy-start.11
  137.2 9.0 %copy-start.3 = (bf16[128,512]{1,0:T(8,128)(2,1)S(1)}, bf16[128,512]{1,0:T(8,128)(2,1)}, u32[]{:S(2)}) copy-start(bf16[128,512]{1,0:T(8,128)(2,1)} %param.24) | copy-start | bytes 393220
  138.9 14.3 %copy-start.1 = (bf16[512,128]{1,0:T(8,128)(2,1)S(1)}, bf16[512,128]{1,0:T(8,128)(2,1)}, u32[]{:S(2)}) copy-start(bf16[512,128]{1,0:T(8,128)(2,1)} %fusion.24) | copy-start | bytes 393220
  138.9 14.3 %copy-start.8 = (f32[512]{0:T(512)S(1)}, f32[512]{0:T(512)}, u32[]{:S(2)}) copy-start(f32[512]{0:T(512)} %dynamic_slice.29) | copy-start | bytes 6148
  170.7 69.5 %reduce-scatter.2.cloned.1.call-start = ((), (), s32[]{:S(2)}) async-start(), calls=%async_computation.4 | async-start | bytes 2621440 | tf_op jit(solution)/shard_map/reduce_scatter | solution.py:227
  208.8 37.1 %copy-start.12 = (pred[128,2]{0,1:T(4,128)(4,1)S(1)}, pred[128,2]{0,1:T(4,128)(4,1)}, u32[]{:S(2)}) copy-start(pred[128,2]{0,1:T(4,128)(4,1)} %get-tuple-element.164) | copy-start | bytes 772
  208.8 37.3 %copy-start.14 = (f32[128,2]{0,1:T(2,128)S(1)}, f32[128,2]{0,1:T(2,128)}, u32[]{:S(2)}) copy-start(f32[128,2]{0,1:T(2,128)} %param.40) | copy-start | bytes 3076
  208.8 37.3 %copy-start.15 = (f32[128]{0:T(128)S(1)}, f32[128]{0:T(128)}, u32[]{:S(2)}) copy-start(f32[128]{0:T(128)} %param.39) | copy-start | bytes 1540
  240.2 19.8 %all-to-all-start.1 = ((bf16[8,64,512]{2,1,0:T(8,128)(2,1)}), bf16[8,64,512]{2,1,0:T(8,128)(2,1)S(1)}, u32[]{:S(2)}, u32[]{:S(2)}) async-start(bf16[8,64,512]{2,1,0:T(8,128)(2,1)} %reduce-scatter.2.cloned.1.call-done), calls=%async_computation.2 | async-start | bytes 1048576 | tf_op jit(solution)/shard_map/all_to_all | solution.py:231
Sparse Core Ops, SparseCore 0:
  38.3 42.6 all-gather.9
  83.1 38.9 all-gather.11
  170.8 20.9 all-gather.7
  209.0 31.1 reduce-scatter.1
where the time goes:
time: 270 us; the launch traced here: 269 us
  waiting for transfers between devices  132 us (49%)
  blocking collectives  52.3 us (19%)
  matrix products  23.5 us (9%)
  other arithmetic  22.8 us (8%)
  between operations  14.3 us (5%)
  starting transfers between devices  12.8 us (5%)
  local copies, waits for them, and re-layouts  11 us (4%)
    all_gather x2, waiting for transfers between devices, entering(): lax.all_gather(a.astype(kind), axis)  53.1 us
    reduce_scatter x1, waiting for transfers between devices, body(): lax.psum_scatter(partial_out, 'tp', scatter_dimension=2, tiled=True)  31.3 us
    unnamed x1, blocking collectives  21.6 us
    all_gather x1, waiting for transfers between devices, body(): lax.all_gather(lax.all_to_all(outgoing, 'sp', split_axis=0, concat_axis=0...  20.9 us
    all_to_all x1, blocking collectives, body(): lax.all_to_all(outgoing, 'sp', split_axis=0, concat_axis=0, tiled=True)  17.1 us
    all_to_all x1, waiting for transfers between devices, body(): lax.all_to_all(expert_cols, 'sp', split_axis=0, concat_axis=0, tiled=True)  13.7 us
    ppermute x1, waiting for transfers between devices, extended(): lax.ppermute(tail, axis, [(i, (i + 1) % count) for i in range(ends)])  13.3 us
    dot_general x1, matrix products, body(): jnp.dot(hidden, weight_down, preferred_element_type=jnp.float32)  10.5 us
  transfers between devices with their start and end apart: 7, of which 6 were waited for; matrix products, arithmetic and copies ran while one was open for 4% of the time, Pallas kernels for 0%

commit v1 on v0

--- a/solution.py
+++ b/solution.py
@@ -1,6 +1,10 @@
+import functools
+
 import jax
 import jax.numpy as jnp
 from jax import lax
+from jax.experimental import pallas as pl
+from jax.experimental.pallas import tpu as pltpu
 from jax.sharding import PartitionSpec as P
 
 D = 2048
@@ -105,6 +109,341 @@
 
 def compose(earlier, later):
     return (earlier[0] + later[0], earlier[1] * jnp.exp(later[0])[:, None, None] + later[1])
+
+
+MESH = pl.DeviceIdType.MESH
+F32 = jnp.float32
+BF16 = jnp.bfloat16
+
+
+def remote(src, dst, send, recv, device):
+    return pltpu.make_async_remote_copy(
+        src_ref=src, dst_ref=dst, send_sem=send, recv_sem=recv, device_id=device, device_id_type=MESH
+    )
+
+
+def expert_kernel(
+    count,
+    tps,
+    cap,
+    stream_ref,
+    selector_ref,
+    high_ref,
+    low_ref,
+    gain_ref,
+    gate_hbm,
+    up_hbm,
+    down_hbm,
+    out_ref,
+    gate_ref,
+    up_ref,
+    down_ref,
+    leaving,
+    rows,
+    hidden,
+    part,
+    pair_in,
+    pair_out,
+    ring_in,
+    answer,
+    returned,
+    weight_sem,
+    a_send,
+    a_recv,
+    b_send,
+    b_recv,
+    p_send,
+    p_recv,
+    q_send,
+    q_recv,
+    r_send,
+    r_recv,
+):
+    me = lax.axis_index("sp")
+    mine = lax.axis_index("tp")
+    halves = tps // 2
+    tall = mine // 2
+    core = mine % 2
+    mate = tall * 2 + (1 - core)
+    cols = stream_ref.shape[1]
+    loads = [
+        pltpu.make_async_copy(gate_hbm.at[0], gate_ref, weight_sem.at[0]),
+        pltpu.make_async_copy(up_hbm.at[0], up_ref, weight_sem.at[1]),
+        pltpu.make_async_copy(down_hbm.at[0], down_ref, weight_sem.at[2]),
+    ]
+    for load in loads:
+        load.start()
+
+    barrier = pltpu.get_barrier_semaphore()
+    for k in range(1, count):
+        pl.semaphore_signal(
+            barrier, inc=1, device_id={"sp": (me + k) % count, "tp": mine}, device_id_type=MESH
+        )
+    for j in range(1, tps):
+        pl.semaphore_signal(
+            barrier, inc=1, device_id={"sp": me, "tp": (mine + j) % tps}, device_id_type=MESH
+        )
+    stream = stream_ref[...]
+    sent = jnp.dot(selector_ref[...], stream, preferred_element_type=F32).astype(BF16)
+    leaving[...] = sent
+    rows[mine, 0:cap, :] = sent[0:cap]
+    pl.semaphore_wait(barrier, count + tps - 2)
+
+    pending = []
+
+    def go(copy):
+        copy.start()
+        pending.append(copy)
+
+    for k in range(1, count):
+        go(
+            remote(
+                leaving.at[pl.ds(k * cap, cap), :],
+                rows.at[mine, pl.ds(k * cap, cap), :],
+                a_send.at[k],
+                a_recv.at[k],
+                {"sp": (me + k) % count, "tp": mine},
+            )
+        )
+
+    batches = min(count, 8)
+    span = count // batches
+
+    def area(owner, batch):
+        return rows.at[owner, pl.ds(batch * span * cap, span * cap), :]
+
+    def arrived_from(owner, batch, index):
+        remote(
+            area(owner, batch),
+            area(owner, batch),
+            b_send.at[index, batch],
+            b_recv.at[index, batch],
+            {"tp": mate},
+        ).wait_recv()
+
+    def relay(batch):
+        for j in range(1, halves):
+            owner = ((tall + halves - j) % halves) * 2 + core
+            arrived_from(owner, batch, j)
+            go(
+                remote(
+                    area(owner, batch),
+                    area(owner, batch),
+                    b_send.at[halves + j, batch],
+                    b_recv.at[halves + j, batch],
+                    {"tp": mate},
+                )
+            )
+
+    for batch in range(batches):
+        for k in range(batch * span, (batch + 1) * span):
+            if k > 0:
+                spot = rows.at[mine, pl.ds(k * cap, cap), :]
+                remote(spot, spot, a_send.at[k], a_recv.at[k], {"tp": mate}).wait_recv()
+        for j in range(1, halves):
+            go(
+                remote(
+                    area(mine, batch),
+                    area(mine, batch),
+                    b_send.at[j, batch],
+                    b_recv.at[j, batch],
+                    {"tp": ((tall + j) % halves) * 2 + core},
+                )
+            )
+        go(
+            remote(
+                area(mine, batch),
+                area(mine, batch),
+                b_send.at[halves, batch],
+                b_recv.at[halves, batch],
+                {"tp": mate},
+            )
+        )
+        if batch > 0:
+            relay(batch - 1)
+    relay(batches - 1)
+    for batch in range(batches):
+        for j in range(halves):
+            arrived_from(((tall + halves - j) % halves) * 2 + 1 - core, batch, halves + j)
+    for copy in pending:
+        copy.wait_send()
+    pending = []
+
+    chunks = 2
+    size = count * cap // chunks
+    units = gate_ref.shape[1]
+    tile = min(256, units)
+    for load in loads:
+        load.wait()
+
+    def compute(chunk):
+        lo = chunk * size
+        squares = jnp.zeros((size, 1), F32)
+        for t in range(tps):
+            piece = rows[t, lo : lo + size, :].astype(F32)
+            squares = squares + jnp.sum(piece * piece, axis=1, keepdims=True)
+        scale = lax.rsqrt(squares / (tps * cols) + stream_eps)
+        for t in range(tps):
+            piece = rows[t, lo : lo + size, :].astype(F32)
+            gain = gain_ref[:, t * cols : (t + 1) * cols]
+            rows[t, lo : lo + size, :] = (piece * scale * gain).astype(BF16)
+
+        @pl.loop(0, units // tile)
+        def _(step):
+            where = pl.ds(pl.multiple_of(step * tile, tile), tile)
+            gate = jnp.zeros((size, tile), F32)
+            upward = jnp.zeros((size, tile), F32)
+            for t in range(tps):
+                piece = rows[t, lo : lo + size, :]
+                ins = slice(t * cols, (t + 1) * cols)
+                gate = gate + jnp.dot(piece, gate_ref[ins, where], preferred_element_type=F32)
+                upward = upward + jnp.dot(piece, up_ref[ins, where], preferred_element_type=F32)
+            hidden[:, where] = (jax.nn.silu(gate) * upward).astype(BF16)
+
+        @pl.loop(0, tps)
+        def _(t):
+            where = pl.ds(pl.multiple_of(t * cols, cols), cols)
+            done = jnp.dot(hidden[...], down_ref[:, where], preferred_element_type=F32)
+            part[chunk, t % 2, t // 2] = done.astype(BF16)
+
+    def pair_copy(chunk):
+        return remote(
+            part.at[chunk, 1 - core],
+            pair_in.at[chunk],
+            p_send.at[chunk],
+            p_recv.at[chunk],
+            {"tp": mate},
+        )
+
+    def cross_copy(chunk, j):
+        return remote(
+            pair_out.at[chunk, j - 1],
+            ring_in.at[chunk, j - 1],
+            q_send.at[chunk, j - 1],
+            q_recv.at[chunk, j - 1],
+            {"tp": ((tall + j) % halves) * 2 + core},
+        )
+
+    def cross(chunk):
+        pair_copy(chunk).wait_recv()
+        for j in range(1, halves):
+            to = (tall + j) % halves
+            total = part[chunk, core, to].astype(F32) + pair_in[chunk, to].astype(F32)
+            pair_out[chunk, j - 1] = total.astype(BF16)
+            go(cross_copy(chunk, j))
+
+    def send_back(chunk):
+        total = part[chunk, core, tall].astype(F32) + pair_in[chunk, tall].astype(F32)
+        for j in range(1, halves):
+            cross_copy(chunk, j).wait_recv()
+            total = total + ring_in[chunk, j - 1].astype(F32)
+        total = total.astype(BF16)
+        each = count // chunks
+        if chunk == 0:
+            returned[0:cap, :] = total[0:cap]
+        answer[chunk * size : (chunk + 1) * size, :] = total
+        for k in range(chunk * each, (chunk + 1) * each):
+            if k > 0:
+                go(back_copy(k))
+
+    def back_copy(k):
+        return remote(
+            answer.at[pl.ds(k * cap, cap), :],
+            returned.at[pl.ds(k * cap, cap), :],
+            r_send.at[k],
+            r_recv.at[k],
+            {"sp": (me + count - k) % count, "tp": mine},
+        )
+
+    for chunk in range(chunks):
+        compute(chunk)
+        go(pair_copy(chunk))
+        if chunk > 0:
+            send_back(chunk - 1)
+        cross(chunk)
+    send_back(chunks - 1)
+    for k in range(1, count):
+        back_copy(k).wait_recv()
+    back = returned[...]
+    total = jnp.dot(high_ref[...], back, preferred_element_type=F32)
+    total = total + jnp.dot(low_ref[...], back, preferred_element_type=F32)
+    out_ref[...] = (stream.astype(F32) + total).astype(BF16)
+    for copy in pending:
+        copy.wait_send()
+
+
+def experts(stream, selector, high, low, gain, gate, up, down, cap):
+    count = lax.axis_size("sp")
+    tps = lax.axis_size("tp")
+    halves = tps // 2
+    tokens, cols = stream.shape
+    slots = count * cap
+    size = slots // 2
+    batches = min(count, 8)
+    vm = pl.BlockSpec(memory_space=pltpu.VMEM)
+    hbm = pl.BlockSpec(memory_space=pl.ANY)
+    dma = pltpu.SemaphoreType.DMA
+    return pl.pallas_call(
+        functools.partial(expert_kernel, count, tps, cap),
+        out_shape=jax.ShapeDtypeStruct((tokens, cols), BF16),
+        in_specs=[vm] * 5 + [hbm] * 3,
+        out_specs=vm,
+        scratch_shapes=[
+            pltpu.VMEM(gate.shape[1:], BF16),
+            pltpu.VMEM(up.shape[1:], BF16),
+            pltpu.VMEM(down.shape[1:], BF16),
+            pltpu.VMEM((slots, cols), BF16),
+            pltpu.VMEM((tps, slots, cols), BF16),
+            pltpu.VMEM((size, gate.shape[2]), BF16),
+            pltpu.VMEM((2, 2, halves, size, cols), BF16),
+            pltpu.VMEM((2, halves, size, cols), BF16),
+            pltpu.VMEM((2, halves - 1, size, cols), BF16),
+            pltpu.VMEM((2, halves - 1, size, cols), BF16),
+            pltpu.VMEM((slots, cols), BF16),
+            pltpu.VMEM((slots, cols), BF16),
+            dma((3,)),
+            dma((count,)),
+            dma((count,)),
+            dma((tps, batches)),
+            dma((tps, batches)),
+            dma((2,)),
+            dma((2,)),
+            dma((2, halves - 1)),
+            dma((2, halves - 1)),
+            dma((count,)),
+            dma((count,)),
+        ],
+        compiler_params=pltpu.CompilerParams(
+            collective_id=1, has_side_effects=True, vmem_limit_bytes=50 * 2**20
+        ),
+        name="experts",
+    )(stream, selector, high, low, gain, gate, up, down)
+
+
+def routes(couple, likelihood, scores, expert_total, capacity):
+    tokens, top = couple.shape
+    place = lax.axis_index("sp")
+    turned = (couple + expert_total - place) % expert_total
+    iota = lax.broadcasted_iota(jnp.int32, (tokens, top, expert_total), 2)
+    hit = turned[:, :, None] == iota
+    named = jnp.sum(hit.astype(jnp.float32), axis=1)
+    lower = jnp.tril(jnp.ones((tokens, tokens), jnp.float32), -1)
+    before = jnp.dot(lower, named, preferred_element_type=jnp.float32).astype(jnp.int32)
+    rank = jnp.sum(jnp.where(hit, before[:, None, :], 0), axis=2)
+    slot = turned * capacity + rank
+    first = jax.nn.sigmoid(scores[:, 0] - scores[:, 1])
+    weight = likelihood[:, None] * jnp.stack([first, 1.0 - first], axis=1)
+    slots = expert_total * capacity
+    lanes = lax.broadcasted_iota(jnp.int32, (tokens, slots), 1)
+    mix = jnp.zeros((tokens, slots), jnp.float32)
+    for k in range(top):
+        mix = mix + jnp.where(slot[:, k : k + 1] == lanes, weight[:, k : k + 1], 0.0)
+    high = mix.astype(jnp.bfloat16)
+    low = (mix - high.astype(jnp.float32)).astype(jnp.bfloat16)
+    column = lax.broadcasted_iota(jnp.int32, (slots, tokens), 0)
+    flat = jnp.transpose(slot)
+    chosen = (flat[0:1] == column) | (flat[1:2] == column)
+    return chosen.astype(jnp.bfloat16), high, low
 
 
 def body(
@@ -181,64 +520,26 @@
         preferred_element_type=jnp.float32,
     )
     stream = (skip_stream_entering.astype(jnp.float32) + projected).astype(jnp.bfloat16)
-    stream_f = stream.astype(jnp.float32)
-    col_count = skip_stream_entering.shape[1]
-    squares = lax.psum(jnp.sum(stream_f * stream_f, axis=1), "tp")
-    row_scale = lax.rsqrt(squares / D + stream_eps)
-    gain_cols = lax.dynamic_slice_in_dim(
-        specialist_rescale_factor, lax.axis_index("tp") * col_count, col_count, 0
-    )
-    normal_cols = (stream_f * row_scale[:, None] * gain_cols).astype(jnp.bfloat16)
     expert_total = lax.axis_size("sp")
     capacity = 4 * tokens_here // expert_total
-    flat_ids = item_specialist_couple.reshape(-1)
-    assignments = flat_ids.shape[0]
-    expert_iota = lax.broadcasted_iota(jnp.int32, (assignments, expert_total), 1)
-    one_hot = (flat_ids[:, None] == expert_iota).astype(jnp.int32)
-    ranking = jnp.sum((jnp.cumsum(one_hot, axis=0) - 1) * one_hot, axis=1)
-    slot_index = flat_ids * capacity + ranking
-    slot_iota = lax.broadcasted_iota(jnp.int32, (expert_total * capacity, assignments), 0)
-    selector = (slot_index[None, :] == slot_iota).astype(jnp.bfloat16)
-    selector = jnp.sum(selector.reshape(expert_total * capacity, tokens_here, -1), axis=2)
-    weight_gate = specialist_gating_weights[0]
-    weight_up = specialist_raising_weights[0]
-    weight_down = specialist_lowering_weights[0]
-    outgoing = jnp.dot(selector, normal_cols, preferred_element_type=jnp.float32).astype(
-        jnp.bfloat16
-    )
-    outgoing = outgoing.reshape(expert_total, capacity, col_count)
-    arrived = lax.all_gather(
-        lax.all_to_all(outgoing, "sp", split_axis=0, concat_axis=0, tiled=True),
-        "tp",
-        axis=2,
-        tiled=True,
-    )
-    sources = arrived.shape[0]
-    slot_count = arrived.shape[1]
-    rows = arrived.reshape(sources * slot_count, arrived.shape[2])
-    gate = jnp.dot(rows, weight_gate, preferred_element_type=jnp.float32)
-    upward = jnp.dot(rows, weight_up, preferred_element_type=jnp.float32)
-    hidden = (jax.nn.silu(gate) * upward).astype(jnp.bfloat16)
-    partial_out = jnp.dot(hidden, weight_down, preferred_element_type=jnp.float32).astype(
-        jnp.bfloat16
-    )
-    partial_out = partial_out.reshape(sources, slot_count, partial_out.shape[1])
-    expert_cols = (
-        lax.psum_scatter(partial_out, "tp", scatter_dimension=2, tiled=True)
-        .astype(jnp.float32)
-        .astype(jnp.bfloat16)
-    )
-    returned = lax.all_to_all(expert_cols, "sp", split_axis=0, concat_axis=0, tiled=True)
-    flat_back = returned.reshape(expert_total * capacity, col_count)
-    picked = (
-        jnp.take(flat_back, slot_index, axis=0)
-        .astype(jnp.float32)
-        .reshape(tokens_here, -1, col_count)
-    )
-    first = jax.nn.sigmoid(selected_twin_scores_raw[:, 0] - selected_twin_scores_raw[:, 1])
-    route_weight = selected_cluster_likelihood[:, None] * jnp.stack([first, 1.0 - first], axis=1)
-    experts_sum = jnp.sum(route_weight[:, :, None] * picked, axis=1)
-    return (stream_f + experts_sum).astype(jnp.bfloat16)
+    selector, high, low = routes(
+        item_specialist_couple,
+        selected_cluster_likelihood,
+        selected_twin_scores_raw,
+        expert_total,
+        capacity,
+    )
+    return experts(
+        stream,
+        selector,
+        high,
+        low,
+        specialist_rescale_factor[None, :],
+        specialist_gating_weights,
+        specialist_raising_weights,
+        specialist_lowering_weights,
+        capacity,
+    )
 
 
 def solution(mesh):

time: 270 us -> 209 us (0.77)
  waiting for transfers between devices: 132 us -> 69.9 us
  Pallas kernels: 0 us -> 57.8 us
  blocking collectives: 52.3 us -> 28.9 us
  matrix products: 23.5 us -> 6.27 us
  other arithmetic: 22.8 us -> 14.9 us
  starting transfers between devices: 12.8 us -> 6.97 us
    pallas_call x0 -> x1, Pallas kernels: none -> 57.8 us  [experts(): pl.pallas_call(functools.partial(expert_kernel, count, tps, cap), out_sha...]
    reduce_scatter x1 -> x0, waiting for transfers between devices: 31.3 us -> none  [body(): lax.psum_scatter(partial_out, 'tp', scatter_dimension=2, tiled=True)]
    all_gather x1 -> x0, waiting for transfers between devices: 20.9 us -> none  [body(): lax.all_gather(lax.all_to_all(outgoing, 'sp', split_axis=0, concat_axis=0...]
    dot_general x3 -> x1, matrix products: 17.4 us -> 0.2 us  [routes(): jnp.dot(lower, named, preferred_element_type=jnp.float32).astype(jnp.int32)]
    all_to_all x1 -> x0, blocking collectives: 17.1 us -> none  [body(): lax.all_to_all(outgoing, 'sp', split_axis=0, concat_axis=0, tiled=True)]
    all_to_all x1 -> x0, waiting for transfers between devices: 13.7 us -> none  [body(): lax.all_to_all(expert_cols, 'sp', split_axis=0, concat_axis=0, tiled=True)]
    psum x1 -> x0, blocking collectives: 6.43 us -> none  [body(): squares = lax.psum(jnp.sum(stream_f * stream_f, axis=1), 'tp')]
    all_to_all x1 -> x0, starting transfers between devices: 5.51 us -> none  [body(): lax.all_to_all(expert_cols, 'sp', split_axis=0, concat_axis=0, tiled=True)]
  transfers between devices with their start and end apart: 7 -> 4, of which waited for: 6 -> 3; matrix products, arithmetic and copies ran while one was open for 4% -> 3% of each run, Pallas kernels for 0% -> 0%
where the time goes in v1:
time: 209 us
  waiting for transfers between devices  69.9 us (33%)
  Pallas kernels  57.8 us (28%)
  blocking collectives  28.9 us (14%)
  other arithmetic  14.9 us (7%)
  between operations  14.6 us (7%)
  local copies, waits for them, and re-layouts  9.09 us (4%)
  starting transfers between devices  6.97 us (3%)
  matrix products  6.27 us (3%)
    pallas_call x1, Pallas kernels, experts(): pl.pallas_call(functools.partial(expert_kernel, count, tps, cap), out_sha...  57.8 us
    all_gather x2, waiting for transfers between devices, entering(): lax.all_gather(a.astype(kind), axis)  57.1 us
    unnamed x1, blocking collectives  21.6 us
    ppermute x1, waiting for transfers between devices, extended(): lax.ppermute(tail, axis, [(i, (i + 1) % count) for i in range(ends)])  12.8 us
    all_gather x1, blocking collectives, body(): lax.all_gather(mixed, 'tp', axis=1, tiled=True)  7.34 us
    add x7, other arithmetic, compose(): earlier[1] * jnp.exp(later[0])[:, None, None] + later[1]  7.13 us
    ppermute x1, starting transfers between devices, extended(): lax.ppermute(tail, axis, [(i, (i + 1) % count) for i in range(ends)])  5.62 us
    unnamed x45, local copies, waits for them, and re-layouts  5.27 us
  transfers between devices with their start and end apart: 4, of which 3 were waited for; matrix products, arithmetic and copies ran while one was open for 3% of the time, Pallas kernels for 0%

profile of v1, /device:TPU:0, one launch (start us, length us, event | category | flops | bytes accessed | tf_op | source)
XLA Modules:
  0.0 208.7 jit_solution(5837033588348691930)
XLA Ops:
  6.6 1.2 copy.62
  7.8 1.0 copy.63
  8.8 1.0 copy.64
  10.1 5.6 %collective-permute-start = (bf16[2,1536]{0,1:T(8,128)(2,1)S(1)}, bf16[2,1536]{0,1:T(8,128)(2,1)}, u32[]{:S(2)}, u32[]{:S(2)}) collective-permute-start(bf16[2,1536]{0,1:T(8,128)(2,1)S(1)} %get-tuple-element.169), channel_id=1, source_target_pairs={{0,4},{4,8},{8,12},{12,16},{16,20},{20,24},{24,28},{1,5},{5,9},{9,... | collective-permute-start | bytes 18440 | tf_op jit(solution)/shard_map/ppermute | solution.py:29
  15.7 1.3 collective-permute-start.1
  18.9 12.8 %collective-permute-done = bf16[2,1536]{0,1:T(8,128)(2,1)} collective-permute-done((bf16[2,1536]{0,1:T(8,128)(2,1)S(1)}, bf16[2,1536]{0,1:T(8,128)(2,1)}, u32[]{:S(2)}, u32[]{:S(2)}) %collective-permute-start) | collective-permute-done | bytes 6176 | tf_op jit(solution)/shard_map/ppermute | solution.py:29
  31.8 1.6 maximum_maximum_fusion
  33.3 3.4 %multiply_convert_fusion = bf16[128,1536]{0,1:T(8,128)(2,1)S(1)} fusion(bf16[130,1536]{0,1:T(8,128)(2,1)S(1)} %get-tuple-element.168, bf16[130,1536]{0,1:T(8,128)(2,1)S(1)} %get-tuple-element.167, f32[1536]{0:T(1024)S(1)} %get-tuple-element.136, f32[1536]{0:T(1024)S(1)} %get-tuple-element.137, f32[1536]{0:T(1024)S(1)} %get-tuple-element.138, ...), kind=kLoop, calls=%fused_computation.18 | loop fusion | flops 4718592 | bytes 2390016 | tf_op jit(solution)/shard_map/convert_element_type | solution.py:484
  37.0 1.3 convolution_convert_fusion.1
  40.2 21.6 %all-reduce.2 = (bf16[64]{0:T(256)(128)(2,1)S(1)}, bf16[64]{0:T(256)(128)(2,1)S(1)}) all-reduce(bf16[64]{0:T(256)(128)(2,1)S(1)} %dynamic-update-slice.1, bf16[64]{0:T(256)(128)(2,1)S(1)} %dynamic-update-slice), channel_id=4, replica_groups=mesh['sp'=8,'tp'=4] {'sp'}, use_global_device_ids=true, to_apply=%add.1 | all-reduce | flops 128 | bytes 512
  62.2 1.3 convolution_convert_fusion
  65.0 16.0 %all-gather.7.cloned.1.call-done = bf16[64,64,128]{2,1,0:T(8,128)(2,1)} async-done(((bf16[8,64,128]{2,1,0:T(8,128)(2,1)}), bf16[64,64,128]{2,1,0:T(8,128)(2,1)}) %all-gather.7.cloned.1.call-update) | async-done | bytes 1048592 | tf_op jit(solution)/shard_map/all_gather | solution.py:43
  81.0 41.1 %all-gather.9.cloned.1.call-done = bf16[64,64,128]{2,1,0:T(8,128)(2,1)} async-done(((bf16[8,64,128]{2,1,0:T(8,128)(2,1)}), bf16[64,64,128]{2,1,0:T(8,128)(2,1)}) %all-gather.9.cloned.1.call-update) | async-done | bytes 1048592 | tf_op jit(solution)/shard_map/all_gather | solution.py:43
  122.2 7.4 %while.27 = (s32[]{:T(128)}, f32[8,64,128]{2,1,0:T(8,128)S(1)}, s32[]{:T(128)}, bf16[8,8]{1,0:T(8,128)(2,1)S(1)}, bf16[8,8,64,128]{3,2,1,0:T(8,128)(2,1)}, /*index=5*/s32[]{:T(128)}, s32[]{:T(128)}, s32[]{:T(128)}, s32[]{:T(128)}) while((s32[]{:T(128)}, f32[8,64,128]{2,1,0:T(8,128)S(1)}, s32[]{:T(128)}, bf16[8,8]{1,0:T(8,128)(2,1)S(1)}, ...), condition=%wide.region_5.6_spmd, body=%wide.region_4.5_spmd.sunk | while | flops 196622 | bytes 655587 | solution.py:58
  123.3 1.0 convert_add_fusion.5
  124.3 1.0 convert_add_fusion.5
  125.4 1.0 convert_add_fusion.5
  126.4 1.0 convert_add_fusion.5
  129.6 1.0 broadcast_in_dim.95
  130.6 1.1 fusion.1
  131.8 1.1 fusion
  133.7 1.0 fusion.25
  135.4 7.3 %all_gather.29 = bf16[128,2048]{1,0:T(8,128)(2,1)S(1)} all-gather(bf16[128,512]{1,0:T(8,128)(2,1)S(1)} %fusion.10), channel_id=1, replica_groups=mesh['sp'=8,'tp'=4] {'tp'}, dimensions={1}, use_global_device_ids=true | all-gather | bytes 655360 | tf_op jit(solution)/shard_map/all_gather | solution.py:518
  143.5 57.8 %experts.1 = bf16[128,512]{1,0:T(8,128)(2,1)S(1)} custom-call(bf16[128,512]{1,0:T(8,128)(2,1)S(1)} %fusion.4.stream_ref, bf16[512,128]{1,0:T(8,128)(2,1)S(1)} %fusion.13.selector_ref, bf16[128,512]{1,0:T(8,128)(2,1)S(1)} %get-tuple-element.182.high_ref, bf16[128,512]{1,0:T(8,128)(2,1)S(1)} %get-tuple-element.181.low_ref, f32[1,2048]{1,0:T(1,128)S(1)} %bitcast.97, ...), custom_call_target="tpu_custom_call" | custom-call | tf_op jit(solution)/shard_map/experts/pallas_call | solution.py:386
  (105 shorter events, 11.3 us)
Async XLA Ops:
  6.5 136.2 %copy-start = (bf16[2048,512]{1,0:T(8,128)(2,1)S(1)}, bf16[2048,512]{1,0:T(8,128)(2,1)}, u32[]{:S(2)}) copy-start(bf16[2048,512]{1,0:T(8,128)(2,1)} %param.36) | copy-start | bytes 6291460
  6.5 10.5 %copy-start.9 = (f32[2,8,128]{2,1,0:T(8,128)S(1)}, f32[2,8,128]{2,1,0:T(8,128)}, u32[]{:S(2)}) copy-start(f32[2,8,128]{2,1,0:T(8,128)} %param.29) | copy-start | bytes 24580
  6.5 10.5 %copy-start.10 = (f32[2,8,128]{2,1,0:T(8,128)S(1)}, f32[2,8,128]{2,1,0:T(8,128)}, u32[]{:S(2)}) copy-start(f32[2,8,128]{2,1,0:T(8,128)} %param.30) | copy-start | bytes 24580
  6.5 10.5 %copy-start.13 = (f32[2,8]{1,0:T(2,128)S(1)}, f32[2,8]{1,0:T(2,128)}, u32[]{:S(2)}) copy-start(f32[2,8]{1,0:T(2,128)} %param.31) | copy-start | bytes 196
  6.5 74.4 %all-gather.7.cloned.1.call-start = ((), (), s32[]{:S(2)}) async-start(), calls=%async_computation | async-start | bytes 1179648 | tf_op jit(solution)/shard_map/all_gather | solution.py:43
  7.8 10.0 %copy-start.6 = (f32[5,512]{1,0:T(8,128)S(1)}, f32[5,512]{1,0:T(8,128)}, u32[]{:S(2)}) copy-start(f32[5,512]{1,0:T(8,128)} %param.32) | copy-start | bytes 30724
  7.8 10.0 %copy-start.7 = (f32[5,512]{1,0:T(8,128)S(1)}, f32[5,512]{1,0:T(8,128)}, u32[]{:S(2)}) copy-start(f32[5,512]{1,0:T(8,128)} %param.33) | copy-start | bytes 30724
  7.8 10.0 %copy-start.8 = (f32[5,512]{1,0:T(8,128)S(1)}, f32[5,512]{1,0:T(8,128)}, u32[]{:S(2)}) copy-start(f32[5,512]{1,0:T(8,128)} %param.34) | copy-start | bytes 30724
  7.8 10.6 %copy-start.11 = (s32[128,2]{0,1:T(2,128)S(1)}, s32[128,2]{0,1:T(2,128)}, u32[]{:S(2)}) copy-start(s32[128,2]{0,1:T(2,128)} %param.38) | copy-start | bytes 3076
  10.1 21.7 %collective-permute-start = (bf16[2,1536]{0,1:T(8,128)(2,1)S(1)}, bf16[2,1536]{0,1:T(8,128)(2,1)}, u32[]{:S(2)}, u32[]{:S(2)}) collective-permute-start(bf16[2,1536]{0,1:T(8,128)(2,1)S(1)} %get-tuple-element.169), channel_id=1, source_target_pairs={{0,4},{4,8},{8,12},{12,16},{16,20},{20,24},{24,28},{1,5},{5,9},{9,... | collective-permute-start | bytes 18440 | tf_op jit(solution)/shard_map/ppermute | solution.py:29
  15.7 16.0 %collective-permute-start.1 = (bf16[2,1536]{0,1:T(8,128)(2,1)S(1)}, bf16[2,1536]{0,1:T(8,128)(2,1)}, u32[]{:S(2)}, u32[]{:S(2)}) collective-permute-start(bf16[2,1536]{0,1:T(8,128)(2,1)S(1)} %get-tuple-element.170), channel_id=1, source_target_pairs={{4,0},{8,4},{12,8},{16,12},{20,16},{24,20},{28,24},{5,1},{9,5},{13... | collective-permute-start | bytes 18440 | tf_op jit(solution)/shard_map/ppermute | solution.py:31
  36.7 1.8 copy-start.16
  36.8 25.2 %copy-start.14 = (f32[128,2]{0,1:T(2,128)S(1)}, f32[128,2]{0,1:T(2,128)}, u32[]{:S(2)}) copy-start(f32[128,2]{0,1:T(2,128)} %param.40) | copy-start | bytes 3076
  36.8 25.2 %copy-start.15 = (f32[128]{0:T(128)S(1)}, f32[128]{0:T(128)}, u32[]{:S(2)}) copy-start(f32[128]{0:T(128)} %param.39) | copy-start | bytes 1540
  36.8 26.7 %copy-start.2 = (bf16[128,512]{0,1:T(8,128)(2,1)}, bf16[128,512]{0,1:T(8,128)(2,1)S(1)}, u32[]{:S(2)}) copy-start(bf16[128,512]{0,1:T(8,128)(2,1)S(1)} %get-tuple-element.166) | copy-start | bytes 393220
  38.3 83.9 %all-gather.9.cloned.1.call-start = ((), (), s32[]{:S(2)}) async-start(), calls=%async_computation.1 | async-start | bytes 1179648 | tf_op jit(solution)/shard_map/all_gather | solution.py:43
  129.6 3.3 %copy-start.3 = (bf16[128,512]{0,1:T(8,128)(2,1)S(1)}, bf16[128,512]{0,1:T(8,128)(2,1)}, u32[]{:S(2)}) copy-start(bf16[128,512]{0,1:T(8,128)(2,1)} %copy-done.2) | copy-start | bytes 393220
  133.6 1.7 copy-start.4
  133.6 1.7 copy-start.12
  133.7 9.0 %copy-start.5 = (bf16[128,512]{1,0:T(8,128)(2,1)S(1)}, bf16[128,512]{1,0:T(8,128)(2,1)}, u32[]{:S(2)}) copy-start(bf16[128,512]{1,0:T(8,128)(2,1)} %param.24) | copy-start | bytes 393220
  142.8 0.7 copy-start.1
Sparse Core Ops, SparseCore 0:
  38.4 42.5 all-gather.6
  83.1 38.9 all-gather.8

commit v2 on v1

--- a/solution.py
+++ b/solution.py
@@ -7,7 +7,6 @@
 from jax.experimental.pallas import tpu as pltpu
 from jax.sharding import PartitionSpec as P
 
-D = 2048
 HD = 64
 NS = 128
 CONV = 5
@@ -16,99 +15,6 @@
 HIGHEST = lax.Precision.HIGHEST
 group_eps = 1e-05
 stream_eps = 1e-06
-
-
-def extended(cells, sides, width):
-    for axis, dim in sides:
-        count = lax.axis_size(axis)
-        ends = count - 1
-        head = lax.slice_in_dim(cells, 0, width, axis=dim)
-        tail = lax.slice_in_dim(cells, cells.shape[dim] - width, cells.shape[dim], axis=dim)
-        cells = jnp.concatenate(
-            [
-                lax.ppermute(tail, axis, [(i, (i + 1) % count) for i in range(ends)]),
-                cells,
-                lax.ppermute(head, axis, [((i + 1) % count, i) for i in range(ends)]),
-            ],
-            axis=dim,
-        )
-    return cells
-
-
-def entering(shard, axis, join, neutral, backward):
-    count = lax.axis_size(axis)
-    place = lax.axis_index(axis)
-    ahead = count - 1 - place if backward else place
-    gathered = jax.tree.map(
-        lambda a, kind: lax.all_gather(a.astype(kind), axis), shard, (jnp.bfloat16, jnp.bfloat16)
-    )
-    state = jax.tree.map(lambda a, e: jnp.zeros_like(a) + jnp.asarray(e, a.dtype), shard, neutral)
-
-    def one(turn, state):
-        source = count - 1 - turn if backward else turn
-        return join(
-            state,
-            jax.tree.map(
-                lambda a, own: lax.dynamic_index_in_dim(a, source, 0, False).astype(own.dtype),
-                gathered,
-                shard,
-            ),
-        )
-
-    return lax.fori_loop(0, ahead, one, state)
-
-
-def block_parts(x_short, b_short, c_short, step_f, step_b, log_f, log_b):
-    head_count = x_short.shape[1]
-    group_count = b_short.shape[1]
-    per_group = head_count // group_count
-    length = x_short.shape[0]
-    group_scores = jnp.einsum("tgn,sgn->gts", c_short, b_short, preferred_element_type=jnp.float32)
-    x_block = x_short.astype(jnp.float32)
-    b_block = b_short.astype(jnp.float32)
-    c_block = c_short.astype(jnp.float32)
-    scores = jnp.repeat(group_scores, per_group, axis=0)
-    b_head = jnp.repeat(b_block, per_group, axis=1)
-    c_head = jnp.repeat(c_block, per_group, axis=1)
-    forward = jnp.cumsum(log_f, axis=1)
-    backward = jnp.flip(jnp.cumsum(jnp.flip(log_b, 1), axis=1), 1)
-    row_index = lax.broadcasted_iota(jnp.int32, (length, length), 0)
-    col_index = lax.broadcasted_iota(jnp.int32, (length, length), 1)
-    lower_mask = (col_index <= row_index)[None]
-    upper_mask = (col_index >= row_index)[None]
-    decay_fwd = jnp.where(
-        lower_mask, jnp.exp(jnp.minimum(forward[:, :, None] - forward[:, None, :], 0.0)), 0.0
-    )
-    decay_bwd = jnp.where(
-        upper_mask, jnp.exp(jnp.minimum(backward[:, :, None] - backward[:, None, :], 0.0)), 0.0
-    )
-    mixing = scores * (decay_fwd * step_f[:, None, :] + decay_bwd * step_b[:, None, :])
-    within = jnp.einsum("hts,shp->thp", mixing, x_block, precision=HIGHEST)
-    weight_fwd = jnp.exp(forward[:, -1:] - forward) * step_f
-    weight_bwd = jnp.exp(backward[:, :1] - backward) * step_b
-    state_fwd = jnp.einsum("hs,shp,shn->hpn", weight_fwd, x_block, b_head, precision=HIGHEST)
-    state_bwd = jnp.einsum("hs,shp,shn->hpn", weight_bwd, x_block, b_head, precision=HIGHEST)
-    return (
-        within,
-        state_fwd,
-        state_bwd,
-        forward[:, -1],
-        backward[:, 0],
-        jnp.exp(forward),
-        jnp.exp(backward),
-        c_head,
-    )
-
-
-def read_state(c_head, factor, state):
-    return (
-        jnp.einsum("thn,hpn->thp", c_head, state, precision=HIGHEST)
-        * jnp.transpose(factor)[:, :, None]
-    )
-
-
-def compose(earlier, later):
-    return (earlier[0] + later[0], earlier[1] * jnp.exp(later[0])[:, None, None] + later[1])
 
 
 MESH = pl.DeviceIdType.MESH
@@ -420,6 +326,353 @@
     )(stream, selector, high, low, gain, gate, up, down)
 
 
+def mixer_kernel(
+    count,
+    tps,
+    feed_ref,
+    entry_ref,
+    exit_ref,
+    valve_ref,
+    increment_ref,
+    attenuation_ref,
+    speed_ref,
+    feed_filter_ref,
+    entry_filter_ref,
+    exit_filter_ref,
+    rescale_ref,
+    skip_ref,
+    weights_hbm,
+    out_ref,
+    weights_ref,
+    halo,
+    wide,
+    table,
+    states,
+    totals,
+    states_in,
+    totals_in,
+    carried,
+    logs,
+    mixed,
+    weight_sem,
+    h_send,
+    h_recv,
+    s_send,
+    s_recv,
+    t_send,
+    t_recv,
+    m_send,
+    m_recv,
+):
+    me = lax.axis_index("sp")
+    mine = lax.axis_index("tp")
+    tokens, cols = feed_ref.shape
+    heads = increment_ref.shape[1]
+    group_count = cols // NS
+    per = heads // group_count
+    load = pltpu.make_async_copy(weights_hbm, weights_ref, weight_sem)
+    load.start()
+    barrier = pltpu.get_barrier_semaphore()
+    for k in range(1, count):
+        pl.semaphore_signal(
+            barrier, inc=1, device_id={"sp": (me + k) % count, "tp": mine}, device_id_type=MESH
+        )
+    for j in range(1, tps):
+        pl.semaphore_signal(
+            barrier, inc=1, device_id={"sp": me, "tp": (mine + j) % tps}, device_id_type=MESH
+        )
+
+    sources = (feed_ref, entry_ref, exit_ref)
+    filters = (feed_filter_ref, entry_filter_ref, exit_filter_ref)
+    rim = halo.shape[2]
+
+    def halo_copy(i, side):
+        start = tokens - rim if side == 0 else 0
+        to = (me + 1) % count if side == 0 else (me + count - 1) % count
+        return remote(
+            sources[i].at[pl.ds(start, rim), :],
+            halo.at[side, i],
+            h_send.at[side, i],
+            h_recv.at[side, i],
+            {"sp": to, "tp": mine},
+        )
+
+    up_to = me < count - 1
+    down_to = me > 0
+    pl.semaphore_wait(barrier, count + tps - 2)
+
+    @pl.when(up_to)
+    def _():
+        for i in range(3):
+            halo_copy(i, 0).start()
+
+    @pl.when(down_to)
+    def _():
+        for i in range(3):
+            halo_copy(i, 1).start()
+
+    row = lax.broadcasted_iota(jnp.int32, (tokens, tokens), 0)
+    col = lax.broadcasted_iota(jnp.int32, (tokens, tokens), 1)
+    lower = col <= row
+    diagonal = col == row
+    raw = increment_ref[...]
+    step = jnp.maximum(raw, 0.0) + jnp.log1p(jnp.exp(-jnp.abs(raw)))
+    log = -step * speed_ref[...] + attenuation_ref[...]
+    upto = jnp.where(row <= col, 1.0, 0.0).astype(F32)
+    onward = jnp.where(row >= col, 1.0, 0.0).astype(F32)
+    forward = jnp.dot(log[0], upto, precision=HIGHEST, preferred_element_type=F32)
+    backward = jnp.dot(log[1], onward, precision=HIGHEST, preferred_element_type=F32)
+    total_f = forward[:, tokens - 1 : tokens]
+    total_b = backward[:, 0:1]
+    table[...] = jnp.zeros(table.shape, F32)
+    items = (
+        forward,
+        backward,
+        jnp.exp(total_f - forward) * step[0],
+        jnp.exp(total_b - backward) * step[1],
+        jnp.exp(forward),
+        jnp.exp(backward),
+    )
+    pitch = table.shape[0] // 8
+    for q, item in enumerate(items):
+        table[q * pitch : q * pitch + heads, :] = item
+    turned = jnp.transpose(table[...])
+    totals[...] = jnp.zeros(totals.shape, F32)
+    totals[0, 0:heads, :] = jnp.broadcast_to(total_f, (heads, totals.shape[2]))
+    totals[1, 0:heads, :] = jnp.broadcast_to(total_b, (heads, totals.shape[2]))
+    lane_head = lax.broadcasted_iota(jnp.int32, (1, NS), 1) // HD
+
+    def spread(q, g):
+        first = g * per
+        value = turned[:, q * pitch + first : q * pitch + first + 1]
+        for i in range(1, per):
+            at = q * pitch + first + i
+            value = jnp.where(lane_head >= i, turned[:, at : at + 1], value)
+        return value
+
+    halo_zero = jnp.zeros((rim, cols), F32)
+
+    @pl.when(down_to)
+    def _():
+        for i in range(3):
+            halo_copy(i, 0).wait_recv()
+            wide[i, 0:rim, :] = halo[0, i].astype(F32)
+
+    @pl.when(me == 0)
+    def _():
+        for i in range(3):
+            wide[i, 0:rim, :] = halo_zero
+
+    @pl.when(up_to)
+    def _():
+        for i in range(3):
+            halo_copy(i, 1).wait_recv()
+            wide[i, rim + tokens : 2 * rim + tokens, :] = halo[1, i].astype(F32)
+
+    @pl.when(me == count - 1)
+    def _():
+        for i in range(3):
+            wide[i, rim + tokens : 2 * rim + tokens, :] = halo_zero
+
+    short = []
+    for i in range(3):
+        wide[i, rim : rim + tokens, :] = sources[i][...].astype(F32)
+        taps = filters[i][...]
+        summed = jnp.zeros((tokens, cols), F32)
+        for offset in range(CONV):
+            begin = rim - CONV // 2 + offset
+            summed = summed + taps[offset : offset + 1] * wide[i, begin : begin + tokens, :]
+        short.append(jax.nn.silu(summed).astype(BF16))
+    x_all, b_all, c_all = short
+    across = (((0,), (0,)), ((), ()))
+    along = (((1,), (1,)), ((), ()))
+    for g in range(group_count):
+        part = slice(g * NS, (g + 1) * NS)
+        x_group = x_all[:, part].astype(F32)
+        for way in range(2):
+            weighted = (x_group * spread(2 + way, g)).astype(BF16)
+            states[way, g] = lax.dot_general(
+                weighted, b_all[:, part], across, preferred_element_type=F32
+            ).astype(BF16)
+
+    def state_copy(way, k):
+        to = (me + k) % count if way == 0 else (me + count - k) % count
+        return remote(
+            states.at[way],
+            states_in.at[way, k - 1],
+            s_send.at[way, k - 1],
+            s_recv.at[way, k - 1],
+            {"sp": to, "tp": mine},
+        )
+
+    def total_copy(way, k):
+        to = (me + k) % count if way == 0 else (me + count - k) % count
+        return remote(
+            totals.at[way],
+            totals_in.at[way, k - 1],
+            t_send.at[way, k - 1],
+            t_recv.at[way, k - 1],
+            {"sp": to, "tp": mine},
+        )
+
+    def sends(way, k):
+        return me + k < count if way == 0 else me >= k
+
+    def takes(way, k):
+        return sends(1 - way, k)
+
+    for k in range(1, count):
+        for way in range(2):
+
+            @pl.when(sends(way, k))
+            def _(way=way, k=k):
+                total_copy(way, k).start()
+                state_copy(way, k).start()
+
+    within = []
+    for g in range(group_count):
+        part = slice(g * NS, (g + 1) * NS)
+        scores = lax.dot_general(
+            c_all[:, part], b_all[:, part], along, preferred_element_type=F32
+        )
+        whole = None
+        for i in range(per):
+            h = g * per + i
+            gap_f = turned[:, h : h + 1] - forward[h : h + 1, :]
+            gap_b = turned[:, pitch + h : pitch + h + 1] - backward[h : h + 1, :]
+            decay = jnp.exp(jnp.minimum(jnp.where(lower, gap_f, gap_b), 0.0))
+            step_f = step[0, h : h + 1, :]
+            step_b = step[1, h : h + 1, :]
+            decay = decay * jnp.where(lower, step_f, step_b) + jnp.where(diagonal, step_b, 0.0)
+            value = jnp.dot(
+                (scores * decay).astype(BF16), x_all[:, part], preferred_element_type=F32
+            )
+            whole = value if whole is None else jnp.where(lane_head >= i, value, whole)
+        within.append(whole)
+
+    carried[...] = jnp.zeros(carried.shape, F32)
+    logs[...] = jnp.zeros(logs.shape, F32)
+    row_head = lax.broadcasted_iota(jnp.int32, (NS, 1), 0) // HD
+    for k in range(1, count):
+        for way in range(2):
+
+            @pl.when(takes(way, k))
+            def _(way=way, k=k):
+                total_copy(way, k).wait_recv()
+                state_copy(way, k).wait_recv()
+                factor = jnp.exp(logs[way])
+                for g in range(group_count):
+                    scale = factor[g * per : g * per + 1, :]
+                    for i in range(1, per):
+                        at = g * per + i
+                        scale = jnp.where(row_head >= i, factor[at : at + 1, :], scale)
+                    carried[way, g] += states_in[way, k - 1, g].astype(F32) * scale
+                logs[way] += totals_in[way, k - 1]
+
+    for g in range(group_count):
+        part = slice(g * NS, (g + 1) * NS)
+        value = within[g]
+        for way in range(2):
+            read = lax.dot_general(
+                c_all[:, part], carried[way, g].astype(BF16), along, preferred_element_type=F32
+            )
+            value = value + read * spread(4 + way, g)
+        value = value * jax.nn.silu(valve_ref[:, part].astype(F32))
+        value = value * lax.rsqrt(jnp.mean(value * value, axis=-1, keepdims=True) + group_eps)
+        mixed[mine, :, part] = (value * rescale_ref[:, part]).astype(BF16)
+
+    def mixed_copy(j):
+        return remote(
+            mixed.at[mine],
+            mixed.at[mine],
+            m_send.at[j - 1],
+            m_recv.at[j - 1],
+            {"sp": me, "tp": (mine + j) % tps},
+        )
+
+    for j in range(1, tps):
+        mixed_copy(j).start()
+    load.wait()
+
+    def product(owner):
+        ins = pl.ds(pl.multiple_of(owner * cols, cols), cols)
+        return jnp.dot(mixed[owner], weights_ref[ins, :], preferred_element_type=F32)
+
+    result = skip_ref[...].astype(F32) + product(mine)
+    for j in range(1, tps):
+        owner = (mine + tps - j) % tps
+        spot = mixed.at[owner]
+        remote(
+            spot, spot, m_send.at[j - 1], m_recv.at[j - 1], {"sp": me, "tp": owner}
+        ).wait_recv()
+        result = result + product(owner)
+    out_ref[...] = result.astype(BF16)
+
+    for j in range(1, tps):
+        mixed_copy(j).wait_send()
+    for k in range(1, count):
+        for way in range(2):
+
+            @pl.when(sends(way, k))
+            def _(way=way, k=k):
+                total_copy(way, k).wait_send()
+                state_copy(way, k).wait_send()
+
+    @pl.when(up_to)
+    def _():
+        for i in range(3):
+            halo_copy(i, 0).wait_send()
+
+    @pl.when(down_to)
+    def _():
+        for i in range(3):
+            halo_copy(i, 1).wait_send()
+
+
+def mixer(feed, entry, leave, valve, inc, att, speed, taps, rescale, skip, weights):
+    count = lax.axis_size("sp")
+    tps = lax.axis_size("tp")
+    tokens, cols = feed.shape
+    group_count = cols // NS
+    vm = pl.BlockSpec(memory_space=pltpu.VMEM)
+    hbm = pl.BlockSpec(memory_space=pl.ANY)
+    dma = pltpu.SemaphoreType.DMA
+    rim = 16
+    pitch = 16
+    return pl.pallas_call(
+        functools.partial(mixer_kernel, count, tps),
+        out_shape=jax.ShapeDtypeStruct((tokens, cols), BF16),
+        in_specs=[vm] * 12 + [hbm],
+        out_specs=vm,
+        scratch_shapes=[
+            pltpu.VMEM(weights.shape, BF16),
+            pltpu.VMEM((2, 3, rim, cols), BF16),
+            pltpu.VMEM((3, tokens + 2 * rim, cols), F32),
+            pltpu.VMEM((8 * pitch, tokens), F32),
+            pltpu.VMEM((2, group_count, NS, NS), BF16),
+            pltpu.VMEM((2, pitch, NS), F32),
+            pltpu.VMEM((2, count - 1, group_count, NS, NS), BF16),
+            pltpu.VMEM((2, count - 1, pitch, NS), F32),
+            pltpu.VMEM((2, group_count, NS, NS), F32),
+            pltpu.VMEM((2, pitch, NS), F32),
+            pltpu.VMEM((tps, tokens, cols), BF16),
+            dma,
+            dma((2, 3)),
+            dma((2, 3)),
+            dma((2, count - 1)),
+            dma((2, count - 1)),
+            dma((2, count - 1)),
+            dma((2, count - 1)),
+            dma((tps - 1,)),
+            dma((tps - 1,)),
+        ],
+        compiler_params=pltpu.CompilerParams(
+            collective_id=2, has_side_effects=True, vmem_limit_bytes=40 * 2**20
+        ),
+        name="mixer",
+    )(feed, entry, leave, valve, inc, att, speed, *taps, rescale, skip, weights)
+
+
 def routes(couple, likelihood, scores, expert_total, capacity):
     tokens, top = couple.shape
     place = lax.axis_index("sp")
@@ -469,57 +722,19 @@
     specialist_lowering_weights,
 ):
     tokens_here = skip_stream_entering.shape[0]
-    heads_here = increment_preactivation.shape[1]
-    x_width = unfiltered_channel_feed.shape[1]
-    b_width = unfiltered_state_entry.shape[1]
-    groups_here = b_width // NS
-    joined = jnp.concatenate(
-        [unfiltered_channel_feed, unfiltered_state_entry, unfiltered_state_exit], axis=1
+    stream = mixer(
+        unfiltered_channel_feed,
+        unfiltered_state_entry,
+        unfiltered_state_exit,
+        final_valve_preactivation,
+        increment_preactivation,
+        summed_attenuation_both_ways,
+        channel_fading_speed[:, :, None],
+        (channel_feed_filter, state_entry_filter, state_exit_filter),
+        clustered_rescale_factor[None, :],
+        skip_stream_entering,
+        final_projection_weights,
     )
-    padded = extended(joined, (("sp", 0),), CONV // 2)
-    kernel = jnp.concatenate([channel_feed_filter, state_entry_filter, state_exit_filter], axis=1)
-    summed = jnp.zeros(joined.shape, jnp.float32)
-    for offset in range(CONV):
-        summed = summed + kernel[offset] * padded[offset : offset + tokens_here].astype(jnp.float32)
-    conv_out = jax.nn.silu(summed).astype(jnp.bfloat16)
-    x_conv = conv_out[:, :x_width].reshape(tokens_here, heads_here, HD)
-    b_conv = conv_out[:, x_width : x_width + b_width].reshape(tokens_here, groups_here, NS)
-    c_conv = conv_out[:, x_width + b_width :].reshape(tokens_here, groups_here, NS)
-    whole_increment_list = jax.nn.softplus(increment_preactivation)
-    whole_attenuation_list = (
-        -whole_increment_list * channel_fading_speed[:, :, None] + summed_attenuation_both_ways
-    )
-    within, state_fwd, state_bwd, total_fwd, total_bwd, factor_fwd, factor_bwd, c_head = (
-        block_parts(
-            x_conv,
-            b_conv,
-            c_conv,
-            whole_increment_list[0],
-            whole_increment_list[1],
-            whole_attenuation_list[0],
-            whole_attenuation_list[1],
-        )
-    )
-    empty = (jnp.zeros_like(total_fwd), jnp.zeros_like(state_fwd))
-    incoming_fwd = entering((total_fwd, state_fwd), "sp", compose, empty, False)[1]
-    incoming_bwd = entering((total_bwd, state_bwd), "sp", compose, empty, True)[1]
-    mixer_out = (
-        within
-        + read_state(c_head, factor_fwd, incoming_fwd)
-        + read_state(c_head, factor_bwd, incoming_bwd)
-    )
-    gated = mixer_out.reshape(tokens_here, x_width) * jax.nn.silu(
-        final_valve_preactivation.astype(jnp.float32)
-    )
-    grouped = gated.reshape(tokens_here, groups_here, -1)
-    grouped = grouped * lax.rsqrt(jnp.mean(grouped * grouped, axis=-1, keepdims=True) + group_eps)
-    mixed = (grouped.reshape(tokens_here, x_width) * clustered_rescale_factor).astype(jnp.bfloat16)
-    projected = jnp.dot(
-        lax.all_gather(mixed, "tp", axis=1, tiled=True),
-        final_projection_weights,
-        preferred_element_type=jnp.float32,
-    )
-    stream = (skip_stream_entering.astype(jnp.float32) + projected).astype(jnp.bfloat16)
     expert_total = lax.axis_size("sp")
     capacity = 4 * tokens_here // expert_total
     selector, high, low = routes(

time: 209 us -> 116 us (0.56)
  waiting for transfers between devices: 69.9 us -> 0 us
  Pallas kernels: 57.8 us -> 99.7 us
  blocking collectives: 28.9 us -> 0 us
  between operations: 14.6 us -> 0.07 us
  other arithmetic: 14.9 us -> 3.05 us
  starting transfers between devices: 6.97 us -> 0 us
  matrix products: 6.27 us -> 0.2 us
  local copies, waits for them, and re-layouts: 9.09 us -> 12.5 us
    all_gather x2 -> x0, waiting for transfers between devices: 57.1 us -> none  [entering(): lax.all_gather(a.astype(kind), axis)]
    pallas_call x0 -> x1, Pallas kernels: none -> 42.2 us  [mixer(): pl.pallas_call(functools.partial(mixer_kernel, count, tps), out_shape=jax...]
    unnamed x1 -> x0, blocking collectives: 21.6 us -> none
    ppermute x2 -> x0, waiting for transfers between devices: 12.8 us -> none  [the longest x1 12.8 us: extended(): lax.ppermute(tail, axis, [(i, (i + 1) % count) for i in range(ends)])]
    all_gather x1 -> x0, blocking collectives: 7.34 us -> none  [body(): lax.all_gather(mixed, 'tp', axis=1, tiled=True)]
    add x7 -> x0, other arithmetic: 7.13 us -> none  [compose(): earlier[1] * jnp.exp(later[0])[:, None, None] + later[1]]
    ppermute x2 -> x0, starting transfers between devices: 6.9 us -> none  [the longest x1 5.62 us: extended(): lax.ppermute(tail, axis, [(i, (i + 1) % count) for i in range(ends)])]
    unnamed x45 -> x27, local copies, waits for them, and re-layouts: 5.27 us -> 11.7 us
  transfers between devices with their start and end apart: 4 -> 0, of which waited for: 3 -> 0; matrix products, arithmetic and copies ran while one was open for 3% -> 0% of each run, Pallas kernels for 0% -> 0%
where the time goes in v2:
time: 116 us; the launch traced here: 115 us
  Pallas kernels  99.7 us (86%)
  local copies, waits for them, and re-layouts  12.5 us (11%)
  other arithmetic  3.05 us (3%)
    pallas_call x1, Pallas kernels, experts(): pl.pallas_call(functools.partial(expert_kernel, count, tps, cap), out_sha...  57.5 us
    pallas_call x1, Pallas kernels, mixer(): pl.pallas_call(functools.partial(mixer_kernel, count, tps), out_shape=jax...  42.2 us
    unnamed x27, local copies, waits for them, and re-layouts  11.7 us

profile of v2, /device:TPU:0, one launch (start us, length us, event | category | flops | bytes accessed | tf_op | source)
XLA Modules:
  0.0 115.5 jit_solution(16264371846665942425)
XLA Ops:
  0.0 0.7 and_select_fusion
  0.7 0.8 broadcast_subtract_fusion
  1.5 0.7 maximum_multiply_fusion
  2.1 0.2 convolution_convert_fusion
  2.4 0.7 multiply_add_fusion
  3.1 0.8 copy.24.speed_ref
  3.9 1.6 %copy-done = bf16[2048,512]{1,0:T(8,128)(2,1)S(1)} copy-done((bf16[2048,512]{1,0:T(8,128)(2,1)S(1)}, bf16[2048,512]{1,0:T(8,128)(2,1)}, u32[]{:S(2)}) %copy-start) | copy-done | bytes 2097176
  5.5 0.9 copy-done.1
  6.4 0.9 copy-done.2
  7.3 0.9 copy-done.3
  8.2 0.9 copy-done.4
  9.1 0.9 copy-done.5
  10.0 0.7 copy-done.6
  10.7 0.7 copy-done.7
  11.4 0.7 copy-done.8
  12.1 0.7 copy-done.9
  12.8 0.7 copy-done.10
  13.5 0.7 copy-done.12
  14.2 42.2 %mixer.1.stream_ref = bf16[128,512]{1,0:T(8,128)(2,1)S(1)} custom-call(bf16[128,512]{1,0:T(8,128)(2,1)S(1)} %copy-done.1, bf16[128,512]{1,0:T(8,128)(2,1)S(1)} %copy-done.2, bf16[128,512]{1,0:T(8,128)(2,1)S(1)} %copy-done.3, bf16[128,512]{1,0:T(8,128)(2,1)S(1)} %copy-done.4, f32[2,8,128]{2,1,0:T(8,128)S(1)} %copy-done.9, f32[2,8,128]{2,1,0:T(8,128)S(1)} %copy-done.10, ...), custom_call_target="tpu_custom_call" | custom-call | tf_op jit(solution)/shard_map/mixer/pallas_call | solution.py:642
  56.5 0.1 subtract_convert_fusion
  56.7 0.0 copy-start.11
  56.7 0.7 copy-done.11
  57.4 57.5 %experts.1 = bf16[128,512]{1,0:T(8,128)(2,1)S(1)} custom-call(bf16[128,512]{1,0:T(8,128)(2,1)S(1)} %mixer.1.stream_ref, bf16[512,128]{1,0:T(8,128)(2,1)S(1)} %fusion.2.selector_ref, bf16[128,512]{1,0:T(8,128)(2,1)S(1)} %get-tuple-element.8.high_ref, bf16[128,512]{1,0:T(8,128)(2,1)S(1)} %get-tuple-element.7.low_ref, f32[1,2048]{1,0:T(1,128)S(1)} %bitcast.17, ...), custom_call_target="tpu_custom_call" | custom-call | tf_op jit(solution)/shard_map/experts/pallas_call | solution.py:292
  114.8 0.7 copy.26
  (19 shorter events, 0.1 us)
Async XLA Ops:
  3.9 1.6 %copy-start = (bf16[2048,512]{1,0:T(8,128)(2,1)S(1)}, bf16[2048,512]{1,0:T(8,128)(2,1)}, u32[]{:S(2)}) copy-start(bf16[2048,512]{1,0:T(8,128)(2,1)} %weights_hbm.1) | copy-start | bytes 6291460
  5.5 0.9 copy-start.1
  6.4 0.9 copy-start.2
  7.3 0.9 copy-start.3
  8.2 0.9 copy-start.4
  9.1 0.9 copy-start.5
  10.0 0.7 copy-start.6
  10.7 0.7 copy-start.7
  11.4 0.7 copy-start.8
  12.1 0.7 copy-start.9
  12.8 0.7 copy-start.10
  13.5 0.7 copy-start.12
  56.7 0.7 copy-start.11
